TPU v7x, 32 devices: a whole 2x2x4 slice. The times are simulated.
32 devices in a mesh: kv: 8 (over z, y), tp: 4 (over x, core).
Axes of the slice: x: 2, y: 2, z: 4, core: 2. Of those that a mesh axis runs over, the one named last changes fastest.
Arguments:
- queries: bfloat16 [2, 3072, 1024], P(None, 'kv', 'tp'), may hold values from -112 to 112
- key_states: bfloat16 [2, 3072, 256], P(None, 'kv', 'tp'), may hold values from -4 to 4
- value_states: bfloat16 [2, 3072, 256], P(None, 'kv', 'tp'), may hold values from -6 to 6
- cotangent: bfloat16 [2, 3072, 1024], P(None, 'kv', 'tp'), may hold values from -6 to 6
- gate_logits: float32 [2, 3072, 16], P(None, 'kv', 'tp'), may hold values from -6 to 6
- layer_input: bfloat16 [2, 3072, 4096], P(None, ('kv', 'tp')), may hold values from -6 to 6
- chosen: int32 [2, 48, 4, 16], P(None, 'kv', 'tp'), may hold values from 0 to 47, as said below
Outputs:
- query_grad: bfloat16 [2, 3072, 1024], P(None, 'kv', 'tp')
- key_grad: bfloat16 [2, 3072, 256], P(None, 'kv', 'tp')
- value_grad: bfloat16 [2, 3072, 256], P(None, 'kv', 'tp')
- value_weight_grad: float32 [4096, 256], P(('kv', 'tp'))
Inputs may be any that keep to these rules, and one draw needn't show every extreme that they name: `chosen`: for each sequence, query block b and key head, the 16 entries are distinct blocks; they include b itself and block 0; blocks after b hold only keys after all of the block's queries. Taking the 6 query blocks of one index of kv together (aligned), one sequence and one key head, at most 2 distinct blocks held by any one earlier index of kv are named, and some index reaches 2.
All inputs are finite; a program needn't handle non-finite values.
Results may differ from a plain program's by a relative error of at most 0.0058.
Values may be sent and summed in bfloat16 or wider, within the bound.
A program may use at most 128 MiB of HBM per device.

v0:
```python
import functools
import math

import jax
import jax.numpy as jnp
from jax import lax
from jax.experimental import pallas as pl
from jax.experimental.pallas import tpu as pltpu
from jax.sharding import PartitionSpec as P

BLK = 64
MOST = 2
PAIR = 2
SUB = 8
LANES = 128
NEG = -1e30
MESH = pl.DeviceIdType.MESH
BF = jnp.bfloat16
F32 = jnp.float32


def loop(lo, hi, body):
    def step(i, carry):
        body(i)
        return carry

    lax.fori_loop(lo, hi, step, 0)


def fold(count, body, carry):
    if count <= 8:
        for i in range(count):
            carry = body(i, carry)
        return carry
    return lax.fori_loop(0, count, body, carry)


def at(i, size):
    return pl.ds(i * size, size) if isinstance(i, int) else pl.ds(pl.multiple_of(i * size, size), size)


def whole(
    devs, tps, seqs, own, heads, hd, share, groups,
    chosen_ref, q_ref, c_ref, g_ref, k_ref, v_ref, li_ref,
    dq_ref, kg_ref, vo_ref, wg_ref,
    near_ref, gate_ref, named_ref, hot_ref, asked_ref, farb_ref, nearb_ref,
    reply_ref, far_ref, rows_ref, kt_ref, s_ref, w_ref, ds_ref, dkv_ref,
    out_ref, total_ref, back_ref, vg_ref, acc_ref, part_ref, piece_ref,
    hot_send, hot_recv, far_send, far_recv, li_send, li_recv, li_sem,
    back_send, back_recv, vg_send, vg_recv, piece_send, piece_recv,
):
    me = lax.axis_index("kv")
    my_tp = lax.axis_index("tp")
    toks = own * BLK
    pos = li_ref.shape[1]
    pairs = own // PAIR
    wide = PAIR * BLK
    far_rows = MOST * BLK
    scale = hd**-0.5
    log2e = math.log2(math.e)

    barrier = pltpu.get_barrier_semaphore()
    loop(1, devs, lambda d: pl.semaphore_signal(
        barrier, inc=1, device_id={"kv": lax.rem(me + d, devs)}, device_id_type=MESH
    ))
    for d in range(1, tps):
        pl.semaphore_signal(
            barrier, inc=1, device_id={"tp": lax.rem(my_tp + d, tps)}, device_id_type=MESH
        )

    def ask(m, src):
        return pltpu.make_async_remote_copy(
            src_ref=hot_ref.at[m], dst_ref=asked_ref.at[src],
            send_sem=hot_send.at[m], recv_sem=hot_recv.at[src],
            device_id={"kv": m}, device_id_type=MESH,
        )

    def answer(s, n, src):
        return pltpu.make_async_remote_copy(
            src_ref=reply_ref.at[s, n], dst_ref=far_ref.at[s, src],
            send_sem=far_send.at[s, n], recv_sem=far_recv.at[s, src],
            device_id={"kv": n}, device_id_type=MESH,
        )

    def columns(g, t):
        return at(g * tps + t if groups == devs else t * groups + g, share)

    def shuffle(g, t, src):
        return pltpu.make_async_remote_copy(
            src_ref=li_ref.at[:, :, columns(g, t)],
            dst_ref=rows_ref.at[g, :, at(src, pos), :],
            send_sem=li_send.at[t, g], recv_sem=li_recv.at[src, g],
            device_id={"tp": t}, device_id_type=MESH,
        )

    def keep(g):
        return pltpu.make_async_copy(
            li_ref.at[:, :, columns(g, my_tp)], rows_ref.at[g, :, at(my_tp, pos), :], li_sem.at[g]
        )

    def back(s, m, src):
        return pltpu.make_async_remote_copy(
            src_ref=out_ref.at[s, m], dst_ref=back_ref.at[s, src],
            send_sem=back_send.at[s, m], recv_sem=back_recv.at[s, src],
            device_id={"kv": m}, device_id_type=MESH,
        )

    def spread(s, t, src):
        return pltpu.make_async_remote_copy(
            src_ref=vg_ref.at[s, at(src, hd), :], dst_ref=vg_ref.at[s, at(src, hd), :],
            send_sem=vg_send.at[s, t], recv_sem=vg_recv.at[s, src],
            device_id={"tp": t}, device_id_type=MESH,
        )

    def piece(kv, src):
        return pltpu.make_async_remote_copy(
            src_ref=part_ref.at[kv], dst_ref=piece_ref.at[src],
            send_sem=piece_send.at[kv], recv_sem=piece_recv.at[src],
            device_id={"kv": kv}, device_id_type=MESH,
        )

    peers = [lax.rem(my_tp + d, tps) for d in range(1, tps)]

    count = devs * SUB
    row = lax.broadcasted_iota(jnp.int32, (count, LANES), 0)
    lane = lax.broadcasted_iota(jnp.int32, (devs, LANES), 1)
    holder, inner = row // SUB, row % SUB
    block = jnp.where(inner < own, holder * own + inner, -1)
    topk = chosen_ref.shape[3]
    across = lax.broadcasted_iota(jnp.int32, (count, count), 1)
    down = lax.broadcasted_iota(jnp.int32, (count, count), 0)
    lower = jnp.where((across // SUB == down // SUB) & (across < down), 1.0, 0.0).astype(BF)
    for s in range(seqs):
        seen = jnp.zeros((count, LANES), F32)
        named = []
        for b in range(own):
            hit = jnp.where(block[:, :topk] == chosen_ref[s, b], 1.0, 0.0)
            hit = jnp.broadcast_to(jnp.max(hit, axis=1, keepdims=True), (count, LANES))
            named_ref[s * own + b] = hit.reshape(devs, SUB, LANES)
            named.append(hit)
            seen = jnp.maximum(seen, hit)
        seen = jnp.where(holder < me, seen, 0.0)
        rank = jnp.dot(lower, seen.astype(BF), preferred_element_type=F32)
        for j in range(MOST):
            hot = jnp.where(rank == j, seen, 0.0)
            hot_ref[:, s, j] = hot.reshape(devs, SUB, LANES)
            oks = [jnp.sum((hot * n).reshape(devs, SUB, LANES), axis=1) for n in named]
            for t in range(pairs):
                ok = jnp.where(lane < BLK, oks[PAIR * t], oks[PAIR * t + 1])
                farb_ref[s * pairs + t, j] = (1.0 - ok) * NEG
        for t in range(pairs):
            ok = jnp.where(
                lane[:SUB] < BLK,
                named_ref[s * own + PAIR * t, me],
                named_ref[s * own + PAIR * t + 1, me],
            )
            nearb_ref[s * pairs + t] = (1.0 - ok) * NEG

    pl.semaphore_wait(barrier, devs - 1 + tps - 1)
    loop(0, me, lambda m: ask(m, me).start())
    for t in peers:
        loop(0, groups, lambda g: shuffle(g, t, my_tp).start())
    loop(0, groups, lambda g: keep(g).start())

    for s in range(seqs):
        near_ref[s] = jnp.concatenate([k_ref[s], v_ref[s]], axis=0).T
        gate_ref[s] = jax.nn.sigmoid(g_ref[s]).T

    def blank(m):
        for s in range(seqs):
            far_ref[s, m] = jnp.zeros(far_ref.shape[2:], BF)

    loop(me, devs - 1, blank)

    for s in range(seqs):

        def reply(i):
            n = devs - 1 - i
            if s == 0:
                ask(0, n).wait_recv()
            for j in range(MOST):
                total = None
                for b in range(own):
                    one = asked_ref[n, s, j, b : b + 1, :].astype(BF)
                    term = one * near_ref[s, b * BLK : (b + 1) * BLK, :]
                    total = term if total is None else total + term
                reply_ref[s, n, j * BLK : (j + 1) * BLK, :] = total
            answer(s, n, me).start()

        loop(0, devs - 1 - me, reply)

    chunks = devs - 1
    rows = heads * wide

    def attention(s):
        loop(0, me, lambda m: answer(s, 0, m).wait_recv())

        def turn(m, carry):
            kt_ref[:, at(m, far_rows)] = (far_ref[s, m][:, :hd] * scale).astype(BF).T
            return carry

        fold(chunks, turn, 0)
        for c in range(pairs):
            kt_ref[:, chunks * far_rows + c * wide : chunks * far_rows + (c + 1) * wide] = (
                (near_ref[s, c * wide : (c + 1) * wide, :hd] * scale).astype(BF).T
            )

        for t in range(pairs):
            tok = slice(t * wide, (t + 1) * wide)
            q = (q_ref[s, tok, :].astype(F32) * scale).astype(BF)
            cot = c_ref[s, tok, :].astype(F32)
            gate = gate_ref[s, tok, :]
            zero = jnp.zeros((rows, hd), BF)
            qs = jnp.concatenate([q[:, h * hd : (h + 1) * hd] for h in range(heads)], axis=0)
            bg = jnp.concatenate(
                [gate[:, h : h + 1] * cot[:, h * hd : (h + 1) * hd] for h in range(heads)], axis=0
            ).astype(BF)
            qs = jnp.concatenate([qs, zero], axis=1)
            bg = jnp.concatenate([zero, bg], axis=1)
            dims = (((1,), (1,)), ((), ()))
            ahead = lax.broadcasted_iota(jnp.int32, (wide, rows), 0) <= lax.rem(
                lax.broadcasted_iota(jnp.int32, (wide, rows), 1), wide
            )
            st = s * pairs + t

            def load(kind, c):
                return far_ref[s, c] if kind else near_ref[s, c * wide : (c + 1) * wide, :]

            def place(kind, c):
                return at(c, far_rows) if kind else slice(
                    chunks * far_rows + c * wide, chunks * far_rows + (c + 1) * wide
                )

            def score(kind, c, top):
                kv = load(kind, c)
                raw = lax.dot_general(kv, qs, dims, preferred_element_type=F32) * log2e
                w_ref[place(kind, c), :] = lax.dot_general(kv, bg, dims, preferred_element_type=F32)
                halves = []
                for j in range(MOST if kind else PAIR):
                    if kind:
                        bias = farb_ref[st, j, pl.ds(c, 1), :]
                    else:
                        bias = nearb_ref[st, c * PAIR + j : c * PAIR + j + 1, :]
                    bias = jnp.concatenate([bias] * heads, axis=1)
                    halves.append(raw[j * BLK : (j + 1) * BLK] + bias)
                sc = jnp.concatenate(halves, axis=0)
                if not kind and c == t:
                    sc = jnp.where(ahead, sc, NEG)
                s_ref[place(kind, c), :] = sc
                return jnp.maximum(top, jnp.max(sc.reshape(-1, SUB, rows), axis=0))

            top = jnp.full((SUB, rows), NEG, F32)
            for c in range(t + 1):
                top = score(False, c, top)
            top = fold(chunks, functools.partial(score, True), top)
            top = jnp.max(top, axis=0, keepdims=True)

            def weigh(kind, c, carry):
                norm, dot = carry
                p = jnp.exp2(s_ref[place(kind, c), :] - top)
                s_ref[place(kind, c), :] = p
                norm += jnp.sum(p.reshape(-1, SUB, rows), axis=0)
                dot += jnp.sum((p * w_ref[place(kind, c), :]).reshape(-1, SUB, rows), axis=0)
                return norm, dot

            carry = (jnp.zeros((SUB, rows), F32), jnp.zeros((SUB, rows), F32))
            for c in range(t + 1):
                carry = weigh(False, c, carry)
            norm, dot = fold(chunks, functools.partial(weigh, True), carry)
            inv = 1.0 / jnp.sum(norm, axis=0, keepdims=True)
            dot = jnp.sum(dot, axis=0, keepdims=True) * inv

            def grad(kind, c, carry):
                w = s_ref[place(kind, c), :] * inv
                ds = (w * (w_ref[place(kind, c), :] - dot)).astype(BF)
                ds_ref[place(kind, c), :] = ds
                more = jnp.dot(ds, qs, preferred_element_type=F32)
                more += jnp.dot(w.astype(BF), bg, preferred_element_type=F32)
                if t == 0 or (not kind and c == t):
                    dkv_ref[place(kind, c), :] = more
                else:
                    dkv_ref[place(kind, c), :] += more
                return carry

            for c in range(t + 1):
                grad(False, c, 0)
            fold(chunks, functools.partial(grad, True), 0)
            used = chunks * far_rows + (t + 1) * wide
            dqt = jnp.dot(kt_ref[:, :used], ds_ref[:used, :], preferred_element_type=F32)
            dqt = jnp.concatenate([dqt[:, h * wide : (h + 1) * wide] for h in range(heads)], axis=0)
            dq_ref[s, tok, :] = dqt.T.astype(BF)

        def give(m):
            out_ref[s, m] = dkv_ref[at(m, far_rows), :].astype(BF)
            back(s, m, me).start()

        loop(0, me, give)
        total_ref[s] = dkv_ref[chunks * far_rows :, :]

    loop(0, seqs, attention)

    def product(s, g):
        return jnp.dot(vg_ref[s], rows_ref[g, s], preferred_element_type=F32)

    for t in peers:
        loop(0, groups, lambda g: shuffle(g, t, t).wait_recv())
    loop(0, groups, lambda g: keep(g).wait())
    for s in range(seqs):

        def add(n):
            back(s, 0, n).wait_recv()
            for b in range(own):
                term = None
                for j in range(MOST):
                    one = asked_ref[n, s, j, b : b + 1, :]
                    more = one * back_ref[s, n, j * BLK : (j + 1) * BLK, :].astype(F32)
                    term = more if term is None else term + more
                total_ref[s, b * BLK : (b + 1) * BLK, :] += term

        loop(me + 1, devs, add)
        both = total_ref[s].T.astype(BF)
        kg_ref[s] = both[:hd]
        vo_ref[s] = both[hd:]
        vg_ref[s, at(my_tp, hd), :] = both[hd:]
        for t in peers:
            spread(s, t, my_tp).start()
        if s < seqs - 1:
            for t in peers:
                spread(s, t, t).wait_recv()

            def early(g):
                if s == 0:
                    acc_ref[g] = product(s, g)
                else:
                    acc_ref[g] += product(s, g)

            loop(0, groups, early)

    for t in peers:
        spread(seqs - 1, t, t).wait_recv()

    def final(g):
        last = product(seqs - 1, g)
        return last if seqs == 1 else last + acc_ref[g]

    if groups == devs:

        def stage(i):
            kv = lax.rem(me + 1 + i, devs)
            part_ref[kv] = final(kv).astype(BF)

            @pl.when(i < devs - 1)
            def _():
                piece(kv, me).start()

        loop(0, devs, stage)
    else:
        each = devs // groups

        def stage(g):
            part_ref[pl.ds(g * each, each)] = final(g).T.astype(BF).reshape((each,) + part_ref.shape[1:])

        loop(0, groups, stage)
        loop(0, devs - 1, lambda i: piece(lax.rem(me + 1 + i, devs), me).start())
    piece_ref[me] = part_ref[me]

    def arrive(i):
        piece(0, lax.rem(me + 1 + i, devs)).wait_recv()

    loop(0, devs - 1, arrive)
    result = piece_ref[0].astype(F32)
    for n in range(1, devs):
        result += piece_ref[n].astype(F32)
    wg_ref[...] = result.T if groups == devs else result

    loop(0, me, lambda m: ask(m, me).wait_send())
    for t in peers:
        loop(0, groups, lambda g: shuffle(g, t, my_tp).wait_send())
    for s in range(seqs):
        loop(me + 1, devs, lambda n: answer(s, n, me).wait_send())
        loop(0, me, lambda m: back(s, m, me).wait_send())
        for t in peers:
            spread(s, t, my_tp).wait_send()
    loop(0, devs - 1, lambda i: piece(lax.rem(me + 1 + i, devs), me).wait_send())


def on_device(queries, key_states, value_states, cotangent, gate_logits, layer_input, chosen):
    seqs, toks, width = queries.shape
    hd = key_states.shape[2]
    heads = width // hd
    own = toks // BLK
    pairs = own // PAIR
    devs = lax.axis_size("kv")
    tps = lax.axis_size("tp")
    pos = layer_input.shape[1]
    share = layer_input.shape[2] // (devs * tps)
    groups, cut = devs, share
    if share % LANES:
        groups, cut = devs * share // LANES, LANES
        layer_input = layer_input.reshape(seqs, pos, devs, tps, share)
        layer_input = jnp.swapaxes(layer_input, 2, 3).reshape(seqs, pos, devs * tps * share)
    part = (tps * hd, share) if groups == devs else (share, tps * hd)
    keys = (devs - 1) * MOST * BLK + toks
    rows = heads * PAIR * BLK
    sent = (MOST * BLK, 2 * hd)

    vmem = pl.BlockSpec(memory_space=pltpu.VMEM)
    hbm = pl.BlockSpec(memory_space=pl.ANY)
    dma = pltpu.SemaphoreType.DMA
    query_grad, key_grad, value_grad, weight_grad = pl.pallas_call(
        functools.partial(whole, devs, tps, seqs, own, heads, hd, cut, groups),
        in_specs=[vmem] * 6 + [hbm],
        out_specs=[vmem] * 4,
        out_shape=[
            jax.ShapeDtypeStruct((seqs, toks, width), BF),
            jax.ShapeDtypeStruct((seqs, hd, toks), BF),
            jax.ShapeDtypeStruct((seqs, hd, toks), BF),
            jax.ShapeDtypeStruct((share, tps * hd), F32),
        ],
        scratch_shapes=[
            pltpu.VMEM((seqs, toks, 2 * hd), BF),
            pltpu.VMEM((seqs, toks, heads), F32),
            pltpu.VMEM((seqs * own, devs, SUB, LANES), F32),
            pltpu.VMEM((devs, seqs, MOST, SUB, LANES), F32),
            pltpu.VMEM((devs, seqs, MOST, SUB, LANES), F32),
            pltpu.VMEM((seqs * pairs, MOST, devs, LANES), F32),
            pltpu.VMEM((seqs * pairs, SUB, LANES), F32),
            pltpu.VMEM((seqs, devs) + sent, BF),
            pltpu.VMEM((seqs, devs - 1) + sent, BF),
            pltpu.VMEM((groups, seqs, toks, cut), BF),
            pltpu.VMEM((hd, keys), BF),
            pltpu.VMEM((keys, rows), F32),
            pltpu.VMEM((keys, rows), F32),
            pltpu.VMEM((keys, rows), BF),
            pltpu.VMEM((keys, 2 * hd), F32),
            pltpu.VMEM((seqs, devs - 1) + sent, BF),
            pltpu.VMEM((seqs, toks, 2 * hd), F32),
            pltpu.VMEM((seqs, devs) + sent, BF),
            pltpu.VMEM((seqs, tps * hd, toks), BF),
            pltpu.VMEM((groups, tps * hd, cut), F32),
            pltpu.VMEM((devs,) + part, BF),
            pltpu.VMEM((devs,) + part, BF),
            dma((devs,)), dma((devs,)),
            dma((seqs, devs)), dma((seqs, devs)),
            dma((tps, groups)), dma((tps, groups)), dma((groups,)),
            dma((seqs, devs)), dma((seqs, devs)),
            dma((seqs, tps)), dma((seqs, tps)),
            dma((devs,)), dma((devs,)),
        ],
        compiler_params=pltpu.CompilerParams(
            collective_id=0, has_side_effects=True, vmem_limit_bytes=56 * 2**20
        ),
    )(
        chosen, queries, cotangent, jnp.swapaxes(gate_logits, 1, 2),
        jnp.swapaxes(key_states, 1, 2), jnp.swapaxes(value_states, 1, 2), layer_input,
    )
    return query_grad, jnp.swapaxes(key_grad, 1, 2), jnp.swapaxes(value_grad, 1, 2), weight_grad


def solution(mesh):
    in_specs = (
        P(None, "kv", "tp"),
        P(None, "kv", "tp"),
        P(None, "kv", "tp"),
        P(None, "kv", "tp"),
        P(None, "kv", "tp"),
        P(None, ("kv", "tp"), None),
        P(None, "kv", "tp", None),
    )
    out_specs = (
        P(None, "kv", "tp"),
        P(None, "kv", "tp"),
        P(None, "kv", "tp"),
        P(("kv", "tp"), None),
    )
    return jax.shard_map(
        on_device, mesh=mesh, in_specs=in_specs, out_specs=out_specs, check_vma=False
    )
```

profile of v0, /device:TPU:13, one launch (start us, length us, event | category | flops | bytes accessed | tf_op | source)
XLA Modules:
  0.0 66.0 jit_solution(9969017011822366118)
XLA Ops:
  0.6 58.9 %shard_map.102 = (bf16[2,384,256]{2,1,0:T(8,128)(2,1)}, bf16[2,64,384]{2,1,0:T(8,128)(2,1)}, bf16[2,64,384]{2,1,0:T(8,128)(2,1)}, f32[128,256]{1,0:T(8,128)}) custom-call(s32[2,6,1,16]{3,2,1,0:T(1,128)} %chosen_ref.1, bf16[2,384,256]{2,1,0:T(8,128)(2,1)} %q_ref.1, bf16[2,384,256]{2,1,0:T(8,128)(2,1)} %c_ref.1, f32[2,4,384]{2,1,0:T(4,128)} %bitcast.9, ...), custom_call_target="tpu_custom_call" | custom-call | tf_op jit(solution)/shard_map/pallas_call | solution.py:410
  59.6 1.8 %copy.15 = bf16[2,384,256]{2,1,0:T(8,128)(2,1)} copy(bf16[2,384,256]{2,1,0:T(8,128)(2,1)} %get-tuple-element.16) | data formatting | bytes 786432
  61.3 1.5 %copy.16 = bf16[2,384,64]{1,2,0:T(8,128)(2,1)} copy(bf16[2,384,64]{1,2,0:T(8,128)(2,1)} %bitcast.8) | data formatting | bytes 196608
  62.9 1.5 %copy.17 = bf16[2,384,64]{1,2,0:T(8,128)(2,1)} copy(bf16[2,384,64]{1,2,0:T(8,128)(2,1)} %bitcast.7) | data formatting | bytes 196608
  64.4 1.6 %copy.18 = f32[128,256]{1,0:T(8,128)} copy(f32[128,256]{1,0:T(8,128)} %get-tuple-element.19) | data formatting | bytes 262144
where the time goes:
time: 66.2 us; the launch traced here: 66 us
  Pallas kernels  58.9 us (89%)
  local copies, waits for them, and re-layouts  6.42 us (10%)
    pallas_call x1, Pallas kernels, on_device(): pl.pallas_call(functools.partial(whole, devs, tps, seqs, own, heads, hd,...  58.9 us
    unnamed x4, local copies, waits for them, and re-layouts  6.42 us

commit v1 on v0

--- a/solution.py
+++ b/solution.py
@@ -41,13 +41,14 @@
 
 def whole(
     devs, tps, seqs, own, heads, hd, share, groups,
-    chosen_ref, q_ref, c_ref, g_ref, k_ref, v_ref, li_ref,
-    dq_ref, kg_ref, vo_ref, wg_ref,
+    chosen_ref, q_in, c_in, g_in, k_in, v_in, li_ref,
+    dq_out, kg_out, vo_out, wg_out,
+    q_ref, c_ref, g_ref, k_ref, v_ref, dq_ref, kg_ref, vo_ref, wg_ref,
     near_ref, gate_ref, named_ref, hot_ref, asked_ref, farb_ref, nearb_ref,
     reply_ref, far_ref, rows_ref, kt_ref, s_ref, w_ref, ds_ref, dkv_ref,
     out_ref, total_ref, back_ref, vg_ref, acc_ref, part_ref, piece_ref,
     hot_send, hot_recv, far_send, far_recv, li_send, li_recv, li_sem,
-    back_send, back_recv, vg_send, vg_recv, piece_send, piece_recv,
+    back_send, back_recv, vg_send, vg_recv, piece_send, piece_recv, in_sem, out_sem,
 ):
     me = lax.axis_index("kv")
     my_tp = lax.axis_index("tp")
@@ -118,6 +119,18 @@
             send_sem=piece_send.at[kv], recv_sem=piece_recv.at[src],
             device_id={"kv": kv}, device_id_type=MESH,
         )
+
+    ins = [
+        pltpu.make_async_copy(src, dst, in_sem.at[i])
+        for i, (src, dst) in enumerate(
+            [(k_in, k_ref), (v_in, v_ref), (g_in, g_ref), (q_in, q_ref), (c_in, c_ref)]
+        )
+    ]
+    for copy in ins:
+        copy.start()
+
+    def put(i, src, dst):
+        return pltpu.make_async_copy(src, dst, out_sem.at[i])
 
     peers = [lax.rem(my_tp + d, tps) for d in range(1, tps)]
 
@@ -158,10 +171,9 @@
 
     pl.semaphore_wait(barrier, devs - 1 + tps - 1)
     loop(0, me, lambda m: ask(m, me).start())
-    for t in peers:
-        loop(0, groups, lambda g: shuffle(g, t, my_tp).start())
-    loop(0, groups, lambda g: keep(g).start())
-
+
+    for copy in ins:
+        copy.wait()
     for s in range(seqs):
         near_ref[s] = jnp.concatenate([k_ref[s], v_ref[s]], axis=0).T
         gate_ref[s] = jax.nn.sigmoid(g_ref[s]).T
@@ -188,6 +200,10 @@
             answer(s, n, me).start()
 
         loop(0, devs - 1 - me, reply)
+
+    for t in peers:
+        loop(0, groups, lambda g: shuffle(g, t, my_tp).start())
+    loop(0, groups, lambda g: keep(g).start())
 
     chunks = devs - 1
     rows = heads * wide
@@ -298,6 +314,8 @@
         total_ref[s] = dkv_ref[chunks * far_rows :, :]
 
     loop(0, seqs, attention)
+    puts = [put(0, dq_ref, dq_out)]
+    puts[0].start()
 
     def product(s, g):
         return jnp.dot(vg_ref[s], rows_ref[g, s], preferred_element_type=F32)
@@ -336,8 +354,17 @@
 
             loop(0, groups, early)
 
+    for out in [put(1, kg_ref, kg_out), put(2, vo_ref, vo_out)]:
+        out.start()
+        puts.append(out)
     for t in peers:
         spread(seqs - 1, t, t).wait_recv()
+
+    def other(i):
+        low = devs - 1 - i
+        low = jnp.where(low > me, low, low - 1)
+        high = jnp.where(i < me, i, i + 1)
+        return jnp.where(me * 2 < devs, low, high)
 
     def final(g):
         last = product(seqs - 1, g)
@@ -346,14 +373,12 @@
     if groups == devs:
 
         def stage(i):
-            kv = lax.rem(me + 1 + i, devs)
+            kv = other(i)
             part_ref[kv] = final(kv).astype(BF)
-
-            @pl.when(i < devs - 1)
-            def _():
-                piece(kv, me).start()
-
-        loop(0, devs, stage)
+            piece(kv, me).start()
+
+        loop(0, devs - 1, stage)
+        part_ref[me] = final(me).astype(BF)
     else:
         each = devs // groups
 
@@ -361,17 +386,19 @@
             part_ref[pl.ds(g * each, each)] = final(g).T.astype(BF).reshape((each,) + part_ref.shape[1:])
 
         loop(0, groups, stage)
-        loop(0, devs - 1, lambda i: piece(lax.rem(me + 1 + i, devs), me).start())
+        loop(0, devs - 1, lambda i: piece(other(i), me).start())
     piece_ref[me] = part_ref[me]
 
     def arrive(i):
-        piece(0, lax.rem(me + 1 + i, devs)).wait_recv()
+        piece(0, other(i)).wait_recv()
 
     loop(0, devs - 1, arrive)
     result = piece_ref[0].astype(F32)
     for n in range(1, devs):
         result += piece_ref[n].astype(F32)
     wg_ref[...] = result.T if groups == devs else result
+    puts.append(put(3, wg_ref, wg_out))
+    puts[-1].start()
 
     loop(0, me, lambda m: ask(m, me).wait_send())
     for t in peers:
@@ -381,7 +408,23 @@
         loop(0, me, lambda m: back(s, m, me).wait_send())
         for t in peers:
             spread(s, t, my_tp).wait_send()
-    loop(0, devs - 1, lambda i: piece(lax.rem(me + 1 + i, devs), me).wait_send())
+    loop(0, devs - 1, lambda i: piece(other(i), me).wait_send())
+    for out in puts:
+        out.wait()
+
+
+def leave(count, *refs):
+    ins, outs, held = refs[:count], refs[count : 2 * count], refs[2 * count : 3 * count]
+    sems = refs[3 * count]
+    reads = [pltpu.make_async_copy(ins[i], held[i], sems.at[0, i]) for i in range(count)]
+    writes = [pltpu.make_async_copy(held[i], outs[i], sems.at[1, i]) for i in range(count)]
+    for read in reads:
+        read.start()
+    for read, write in zip(reads, writes):
+        read.wait()
+        write.start()
+    for write in writes:
+        write.wait()
 
 
 def on_device(queries, key_states, value_states, cotangent, gate_logits, layer_input, chosen):
@@ -407,10 +450,10 @@
     vmem = pl.BlockSpec(memory_space=pltpu.VMEM)
     hbm = pl.BlockSpec(memory_space=pl.ANY)
     dma = pltpu.SemaphoreType.DMA
-    query_grad, key_grad, value_grad, weight_grad = pl.pallas_call(
+    results = pl.pallas_call(
         functools.partial(whole, devs, tps, seqs, own, heads, hd, cut, groups),
-        in_specs=[vmem] * 6 + [hbm],
-        out_specs=[vmem] * 4,
+        in_specs=[vmem] + [hbm] * 6,
+        out_specs=[hbm] * 4,
         out_shape=[
             jax.ShapeDtypeStruct((seqs, toks, width), BF),
             jax.ShapeDtypeStruct((seqs, hd, toks), BF),
@@ -418,6 +461,15 @@
             jax.ShapeDtypeStruct((share, tps * hd), F32),
         ],
         scratch_shapes=[
+            pltpu.VMEM((seqs, toks, width), BF),
+            pltpu.VMEM((seqs, toks, width), BF),
+            pltpu.VMEM((seqs, heads, toks), F32),
+            pltpu.VMEM((seqs, hd, toks), BF),
+            pltpu.VMEM((seqs, hd, toks), BF),
+            pltpu.VMEM((seqs, toks, width), BF),
+            pltpu.VMEM((seqs, hd, toks), BF),
+            pltpu.VMEM((seqs, hd, toks), BF),
+            pltpu.VMEM((share, tps * hd), F32),
             pltpu.VMEM((seqs, toks, 2 * hd), BF),
             pltpu.VMEM((seqs, toks, heads), F32),
             pltpu.VMEM((seqs * own, devs, SUB, LANES), F32),
@@ -446,14 +498,23 @@
             dma((seqs, devs)), dma((seqs, devs)),
             dma((seqs, tps)), dma((seqs, tps)),
             dma((devs,)), dma((devs,)),
+            dma((5,)), dma((4,)),
         ],
         compiler_params=pltpu.CompilerParams(
-            collective_id=0, has_side_effects=True, vmem_limit_bytes=56 * 2**20
+            collective_id=0, has_side_effects=True, vmem_limit_bytes=60 * 2**20
         ),
     )(
         chosen, queries, cotangent, jnp.swapaxes(gate_logits, 1, 2),
         jnp.swapaxes(key_states, 1, 2), jnp.swapaxes(value_states, 1, 2), layer_input,
     )
+    query_grad, key_grad, value_grad, weight_grad = pl.pallas_call(
+        functools.partial(leave, len(results)),
+        in_specs=[hbm] * len(results),
+        out_specs=[hbm] * len(results),
+        out_shape=[jax.ShapeDtypeStruct(r.shape, r.dtype) for r in results],
+        scratch_shapes=[pltpu.VMEM(r.shape, r.dtype) for r in results] + [dma((2, len(results)))],
+        compiler_params=pltpu.CompilerParams(vmem_limit_bytes=60 * 2**20),
+    )(*results)
     return query_grad, jnp.swapaxes(key_grad, 1, 2), jnp.swapaxes(value_grad, 1, 2), weight_grad
 
 

time: 66.2 us -> 60.5 us (0.914)
  local copies, waits for them, and re-layouts: 6.42 us -> 0 us
  Pallas kernels: 58.9 us -> 59.7 us
    unnamed x4 -> x0, local copies, waits for them, and re-layouts: 6.42 us -> none
    pallas_call x0 -> x1, Pallas kernels: none -> 1.92 us  [on_device(): pl.pallas_call(functools.partial(leave, len(results)), in_specs=[hbm] * l...]
    pallas_call x1, Pallas kernels: 58.9 us -> 57.8 us  [on_device(): pl.pallas_call(functools.partial(whole, devs, tps, seqs, own, heads, hd,...]
where the time goes in v1:
time: 60.5 us; the launch traced here: 60.4 us
  Pallas kernels  59.7 us (99%)
  between operations  0.64 us (1%)
    pallas_call x1, Pallas kernels, on_device(): pl.pallas_call(functools.partial(whole, devs, tps, seqs, own, heads, hd,...  57.8 us
    pallas_call x1, Pallas kernels, on_device(): pl.pallas_call(functools.partial(leave, len(results)), in_specs=[hbm] * l...  1.92 us

profile of v1, /device:TPU:13, one launch (start us, length us, event | category | flops | bytes accessed | tf_op | source)
XLA Modules:
  0.0 60.4 jit_solution(6355985984772542231)
XLA Ops:
  0.6 57.8 %shard_map.102 = (bf16[2,384,256]{2,1,0:T(8,128)(2,1)}, bf16[2,64,384]{2,1,0:T(8,128)(2,1)}, bf16[2,64,384]{2,1,0:T(8,128)(2,1)}, f32[128,256]{1,0:T(8,128)}) custom-call(s32[2,6,1,16]{3,2,1,0:T(1,128)} %chosen_ref.1, bf16[2,384,256]{2,1,0:T(8,128)(2,1)} %q_in.1, bf16[2,384,256]{2,1,0:T(8,128)(2,1)} %c_in.1, f32[2,4,384]{2,1,0:T(4,128)} %bitcast.7, ...), custom_call_target="tpu_custom_call" | custom-call | tf_op jit(solution)/shard_map/pallas_call | solution.py:453
  58.4 1.9 %shard_map.103 = (bf16[2,384,256]{2,1,0:T(8,128)(2,1)}, bf16[2,64,384]{2,1,0:T(8,128)(2,1)}, bf16[2,64,384]{2,1,0:T(8,128)(2,1)}, f32[128,256]{1,0:T(8,128)}) custom-call(bf16[2,384,256]{2,1,0:T(8,128)(2,1)} %get-tuple-element.12.refs_0_, bf16[2,64,384]{2,1,0:T(8,128)(2,1)} %get-tuple-element.13.refs_1_, bf16[2,64,384]{2,1,0:T(8,128)(2,1)} %get-tuple-element.14.refs_2_, ...), custom_call_target="tpu_custom_call" | custom-call | tf_op jit(solution)/shard_map/pallas_call | solution.py:510

commit v2 on v1

--- a/solution.py
+++ b/solution.py
@@ -27,14 +27,6 @@
     lax.fori_loop(lo, hi, step, 0)
 
 
-def fold(count, body, carry):
-    if count <= 8:
-        for i in range(count):
-            carry = body(i, carry)
-        return carry
-    return lax.fori_loop(0, count, body, carry)
-
-
 def at(i, size):
     return pl.ds(i * size, size) if isinstance(i, int) else pl.ds(pl.multiple_of(i * size, size), size)
 
@@ -45,7 +37,7 @@
     dq_out, kg_out, vo_out, wg_out,
     q_ref, c_ref, g_ref, k_ref, v_ref, dq_ref, kg_ref, vo_ref, wg_ref,
     near_ref, gate_ref, named_ref, hot_ref, asked_ref, farb_ref, nearb_ref,
-    reply_ref, far_ref, rows_ref, kt_ref, s_ref, w_ref, ds_ref, dkv_ref,
+    reply_ref, far_ref, rows_ref, qs_ref, bg_ref, s_ref, w_ref, top_ref, dqt_ref,
     out_ref, total_ref, back_ref, vg_ref, acc_ref, part_ref, piece_ref,
     hot_send, hot_recv, far_send, far_recv, li_send, li_recv, li_sem,
     back_send, back_recv, vg_send, vg_recv, piece_send, piece_recv, in_sem, out_sem,
@@ -178,28 +170,24 @@
         near_ref[s] = jnp.concatenate([k_ref[s], v_ref[s]], axis=0).T
         gate_ref[s] = jax.nn.sigmoid(g_ref[s]).T
 
-    def blank(m):
-        for s in range(seqs):
-            far_ref[s, m] = jnp.zeros(far_ref.shape[2:], BF)
-
-    loop(me, devs - 1, blank)
-
-    for s in range(seqs):
-
-        def reply(i):
-            n = devs - 1 - i
-            if s == 0:
-                ask(0, n).wait_recv()
-            for j in range(MOST):
-                total = None
-                for b in range(own):
-                    one = asked_ref[n, s, j, b : b + 1, :].astype(BF)
-                    term = one * near_ref[s, b * BLK : (b + 1) * BLK, :]
-                    total = term if total is None else total + term
-                reply_ref[s, n, j * BLK : (j + 1) * BLK, :] = total
-            answer(s, n, me).start()
-
-        loop(0, devs - 1 - me, reply)
+    def reply(s, i):
+        n = devs - 1 - i
+        for j in range(MOST):
+            total = None
+            for b in range(own):
+                one = asked_ref[n, s, j, b : b + 1, :].astype(BF)
+                term = one * near_ref[s, b * BLK : (b + 1) * BLK, :]
+                total = term if total is None else total + term
+            reply_ref[s, n, j * BLK : (j + 1) * BLK, :] = total
+        answer(s, n, me).start()
+
+    def first(i):
+        ask(0, devs - 1 - i).wait_recv()
+        reply(0, i)
+
+    later = devs - 1 - me
+    nearest = jnp.minimum(max(devs // 4, 1), later)
+    loop(0, nearest, first)
 
     for t in peers:
         loop(0, groups, lambda g: shuffle(g, t, my_tp).start())
@@ -207,20 +195,31 @@
 
     chunks = devs - 1
     rows = heads * wide
+    dims = (((1,), (1,)), ((), ()))
+    ahead = lax.broadcasted_iota(jnp.int32, (wide, rows), 0) <= lax.rem(
+        lax.broadcasted_iota(jnp.int32, (wide, rows), 1), wide
+    )
+
+    def settle(s):
+        def add(n):
+            back(s, 0, n).wait_recv()
+            for b in range(own):
+                term = None
+                for j in range(MOST):
+                    one = asked_ref[n, s, j, b : b + 1, :]
+                    more = one * back_ref[s, n, j * BLK : (j + 1) * BLK, :].astype(F32)
+                    term = more if term is None else term + more
+                total_ref[s, b * BLK : (b + 1) * BLK, :] += term
+
+        loop(me + 1, devs, add)
+        both = total_ref[s].T.astype(BF)
+        kg_ref[s] = both[:hd]
+        vo_ref[s] = both[hd:]
+        vg_ref[s, at(my_tp, hd), :] = both[hd:]
+        for t in peers:
+            spread(s, t, my_tp).start()
 
     def attention(s):
-        loop(0, me, lambda m: answer(s, 0, m).wait_recv())
-
-        def turn(m, carry):
-            kt_ref[:, at(m, far_rows)] = (far_ref[s, m][:, :hd] * scale).astype(BF).T
-            return carry
-
-        fold(chunks, turn, 0)
-        for c in range(pairs):
-            kt_ref[:, chunks * far_rows + c * wide : chunks * far_rows + (c + 1) * wide] = (
-                (near_ref[s, c * wide : (c + 1) * wide, :hd] * scale).astype(BF).T
-            )
-
         for t in range(pairs):
             tok = slice(t * wide, (t + 1) * wide)
             q = (q_ref[s, tok, :].astype(F32) * scale).astype(BF)
@@ -231,87 +230,105 @@
             bg = jnp.concatenate(
                 [gate[:, h : h + 1] * cot[:, h * hd : (h + 1) * hd] for h in range(heads)], axis=0
             ).astype(BF)
-            qs = jnp.concatenate([qs, zero], axis=1)
-            bg = jnp.concatenate([zero, bg], axis=1)
-            dims = (((1,), (1,)), ((), ()))
-            ahead = lax.broadcasted_iota(jnp.int32, (wide, rows), 0) <= lax.rem(
-                lax.broadcasted_iota(jnp.int32, (wide, rows), 1), wide
+            qs_ref[t] = jnp.concatenate([qs, zero], axis=1)
+            bg_ref[t] = jnp.concatenate([zero, bg], axis=1)
+
+        def score(kv, t, chunk, bias, diagonal, carry):
+            top, norm, dot = carry
+            raw = lax.dot_general(kv, qs_ref[t], dims, preferred_element_type=F32) * log2e
+            wg = lax.dot_general(kv, bg_ref[t], dims, preferred_element_type=F32)
+            sc = jnp.concatenate(
+                [
+                    raw[j * BLK : (j + 1) * BLK] + jnp.concatenate([b] * heads, axis=1)
+                    for j, b in enumerate(bias)
+                ],
+                axis=0,
             )
-            st = s * pairs + t
-
-            def load(kind, c):
-                return far_ref[s, c] if kind else near_ref[s, c * wide : (c + 1) * wide, :]
-
-            def place(kind, c):
-                return at(c, far_rows) if kind else slice(
-                    chunks * far_rows + c * wide, chunks * far_rows + (c + 1) * wide
+            if diagonal:
+                sc = jnp.where(ahead, sc, NEG)
+            peak = jnp.maximum(top, jnp.max(sc, axis=0, keepdims=True))
+            p = jnp.exp2(sc - peak)
+            less = jnp.exp2(top - peak)
+            s_ref[chunk, :, t * rows : (t + 1) * rows] = p.astype(s_ref.dtype)
+            w_ref[chunk, :, t * rows : (t + 1) * rows] = wg
+            top_ref[chunk, :, t * rows : (t + 1) * rows] = peak
+            norm = norm * less + jnp.sum(p, axis=0, keepdims=True)
+            dot = dot * less + jnp.sum(p * wg, axis=0, keepdims=True)
+            return peak, norm, dot
+
+        carries = []
+        for t in range(pairs):
+            carry = (jnp.full((1, rows), NEG, F32), jnp.zeros((1, rows), F32), jnp.zeros((1, rows), F32))
+            for c in range(t, -1, -1):
+                kv = near_ref[s, c * wide : (c + 1) * wide, :]
+                bias = [
+                    nearb_ref[s * pairs + t, c * PAIR + j : c * PAIR + j + 1, :] for j in range(PAIR)
+                ]
+                carry = score(kv, t, chunks + c, bias, c == t, carry)
+            carries.append(carry)
+
+        @pl.when(s == 0)
+        def _():
+            loop(nearest, later, first)
+
+        def forth(i, carries):
+            m = me - 1 - i
+            answer(s, 0, m).wait_recv()
+            kv = far_ref[s, m]
+            return tuple(
+                score(
+                    kv, t, m,
+                    [farb_ref[s * pairs + t, j, pl.ds(m, 1), :] for j in range(MOST)],
+                    False, carries[t],
                 )
-
-            def score(kind, c, top):
-                kv = load(kind, c)
-                raw = lax.dot_general(kv, qs, dims, preferred_element_type=F32) * log2e
-                w_ref[place(kind, c), :] = lax.dot_general(kv, bg, dims, preferred_element_type=F32)
-                halves = []
-                for j in range(MOST if kind else PAIR):
-                    if kind:
-                        bias = farb_ref[st, j, pl.ds(c, 1), :]
-                    else:
-                        bias = nearb_ref[st, c * PAIR + j : c * PAIR + j + 1, :]
-                    bias = jnp.concatenate([bias] * heads, axis=1)
-                    halves.append(raw[j * BLK : (j + 1) * BLK] + bias)
-                sc = jnp.concatenate(halves, axis=0)
-                if not kind and c == t:
-                    sc = jnp.where(ahead, sc, NEG)
-                s_ref[place(kind, c), :] = sc
-                return jnp.maximum(top, jnp.max(sc.reshape(-1, SUB, rows), axis=0))
-
-            top = jnp.full((SUB, rows), NEG, F32)
-            for c in range(t + 1):
-                top = score(False, c, top)
-            top = fold(chunks, functools.partial(score, True), top)
-            top = jnp.max(top, axis=0, keepdims=True)
-
-            def weigh(kind, c, carry):
-                norm, dot = carry
-                p = jnp.exp2(s_ref[place(kind, c), :] - top)
-                s_ref[place(kind, c), :] = p
-                norm += jnp.sum(p.reshape(-1, SUB, rows), axis=0)
-                dot += jnp.sum((p * w_ref[place(kind, c), :]).reshape(-1, SUB, rows), axis=0)
-                return norm, dot
-
-            carry = (jnp.zeros((SUB, rows), F32), jnp.zeros((SUB, rows), F32))
-            for c in range(t + 1):
-                carry = weigh(False, c, carry)
-            norm, dot = fold(chunks, functools.partial(weigh, True), carry)
-            inv = 1.0 / jnp.sum(norm, axis=0, keepdims=True)
-            dot = jnp.sum(dot, axis=0, keepdims=True) * inv
-
-            def grad(kind, c, carry):
-                w = s_ref[place(kind, c), :] * inv
-                ds = (w * (w_ref[place(kind, c), :] - dot)).astype(BF)
-                ds_ref[place(kind, c), :] = ds
-                more = jnp.dot(ds, qs, preferred_element_type=F32)
-                more += jnp.dot(w.astype(BF), bg, preferred_element_type=F32)
-                if t == 0 or (not kind and c == t):
-                    dkv_ref[place(kind, c), :] = more
-                else:
-                    dkv_ref[place(kind, c), :] += more
-                return carry
-
-            for c in range(t + 1):
-                grad(False, c, 0)
-            fold(chunks, functools.partial(grad, True), 0)
-            used = chunks * far_rows + (t + 1) * wide
-            dqt = jnp.dot(kt_ref[:, :used], ds_ref[:used, :], preferred_element_type=F32)
+                for t in range(pairs)
+            )
+
+        carries = lax.fori_loop(0, me, forth, tuple(carries))
+
+        @pl.when((s < seqs - 1) & (me * 2 >= devs))
+        def _():
+            loop(0, later, functools.partial(reply, s + 1))
+
+        @pl.when(s > 0)
+        def _():
+            settle(s - 1)
+
+        tops = [carry[0] for carry in carries]
+        invs = [1.0 / carry[1] for carry in carries]
+        dots = [carry[2] * inv for carry, inv in zip(carries, invs)]
+        dqt_ref[...] = jnp.zeros_like(dqt_ref)
+
+        def grad(kv, chunk, ts):
+            kt = (kv[:, :hd] * scale).astype(BF).T
+            total = None
+            for t in ts:
+                cols = slice(t * rows, (t + 1) * rows)
+                part = jnp.exp2(top_ref[chunk, :, cols] - tops[t]) * invs[t]
+                w = s_ref[chunk, :, cols].astype(F32) * part
+                ds = (w * (w_ref[chunk, :, cols] - dots[t])).astype(BF)
+                more = jnp.dot(ds, qs_ref[t], preferred_element_type=F32)
+                more += jnp.dot(w.astype(BF), bg_ref[t], preferred_element_type=F32)
+                total = more if total is None else total + more
+                dqt_ref[:, cols] += jnp.dot(kt, ds, preferred_element_type=F32)
+            return total
+
+        def give(m):
+            out_ref[s, m] = grad(far_ref[s, m], m, range(pairs)).astype(BF)
+            back(s, m, me).start()
+
+        loop(0, me, give)
+        for c in range(pairs):
+            kv = near_ref[s, c * wide : (c + 1) * wide, :]
+            total_ref[s, c * wide : (c + 1) * wide, :] = grad(kv, chunks + c, range(c, pairs))
+        for t in range(pairs):
+            dqt = dqt_ref[:, t * rows : (t + 1) * rows]
             dqt = jnp.concatenate([dqt[:, h * wide : (h + 1) * wide] for h in range(heads)], axis=0)
-            dq_ref[s, tok, :] = dqt.T.astype(BF)
-
-        def give(m):
-            out_ref[s, m] = dkv_ref[at(m, far_rows), :].astype(BF)
-            back(s, m, me).start()
-
-        loop(0, me, give)
-        total_ref[s] = dkv_ref[chunks * far_rows :, :]
+            dq_ref[s, t * wide : (t + 1) * wide, :] = dqt.T.astype(BF)
+
+        @pl.when((s < seqs - 1) & (me * 2 < devs))
+        def _():
+            loop(0, later, functools.partial(reply, s + 1))
 
     loop(0, seqs, attention)
     puts = [put(0, dq_ref, dq_out)]
@@ -320,39 +337,21 @@
     def product(s, g):
         return jnp.dot(vg_ref[s], rows_ref[g, s], preferred_element_type=F32)
 
+    settle(seqs - 1)
     for t in peers:
         loop(0, groups, lambda g: shuffle(g, t, t).wait_recv())
     loop(0, groups, lambda g: keep(g).wait())
-    for s in range(seqs):
-
-        def add(n):
-            back(s, 0, n).wait_recv()
-            for b in range(own):
-                term = None
-                for j in range(MOST):
-                    one = asked_ref[n, s, j, b : b + 1, :]
-                    more = one * back_ref[s, n, j * BLK : (j + 1) * BLK, :].astype(F32)
-                    term = more if term is None else term + more
-                total_ref[s, b * BLK : (b + 1) * BLK, :] += term
-
-        loop(me + 1, devs, add)
-        both = total_ref[s].T.astype(BF)
-        kg_ref[s] = both[:hd]
-        vo_ref[s] = both[hd:]
-        vg_ref[s, at(my_tp, hd), :] = both[hd:]
+    for s in range(seqs - 1):
         for t in peers:
-            spread(s, t, my_tp).start()
-        if s < seqs - 1:
-            for t in peers:
-                spread(s, t, t).wait_recv()
-
-            def early(g):
-                if s == 0:
-                    acc_ref[g] = product(s, g)
-                else:
-                    acc_ref[g] += product(s, g)
-
-            loop(0, groups, early)
+            spread(s, t, t).wait_recv()
+
+        def early(g):
+            if s == 0:
+                acc_ref[g] = product(s, g)
+            else:
+                acc_ref[g] += product(s, g)
+
+        loop(0, groups, early)
 
     for out in [put(1, kg_ref, kg_out), put(2, vo_ref, vo_out)]:
         out.start()
@@ -443,8 +442,9 @@
         layer_input = layer_input.reshape(seqs, pos, devs, tps, share)
         layer_input = jnp.swapaxes(layer_input, 2, 3).reshape(seqs, pos, devs * tps * share)
     part = (tps * hd, share) if groups == devs else (share, tps * hd)
-    keys = (devs - 1) * MOST * BLK + toks
+    chunks = devs - 1 + pairs
     rows = heads * PAIR * BLK
+    scores = (chunks, PAIR * BLK, pairs * rows)
     sent = (MOST * BLK, 2 * hd)
 
     vmem = pl.BlockSpec(memory_space=pltpu.VMEM)
@@ -480,11 +480,12 @@
             pltpu.VMEM((seqs, devs) + sent, BF),
             pltpu.VMEM((seqs, devs - 1) + sent, BF),
             pltpu.VMEM((groups, seqs, toks, cut), BF),
-            pltpu.VMEM((hd, keys), BF),
-            pltpu.VMEM((keys, rows), F32),
-            pltpu.VMEM((keys, rows), F32),
-            pltpu.VMEM((keys, rows), BF),
-            pltpu.VMEM((keys, 2 * hd), F32),
+            pltpu.VMEM((pairs, rows, 2 * hd), BF),
+            pltpu.VMEM((pairs, rows, 2 * hd), BF),
+            pltpu.VMEM(scores, F32 if math.prod(scores) <= 5 * 2**20 else BF),
+            pltpu.VMEM(scores, F32),
+            pltpu.VMEM((chunks, 1, pairs * rows), F32),
+            pltpu.VMEM((hd, pairs * rows), F32),
             pltpu.VMEM((seqs, devs - 1) + sent, BF),
             pltpu.VMEM((seqs, toks, 2 * hd), F32),
             pltpu.VMEM((seqs, devs) + sent, BF),

time: 60.5 us -> 53.9 us (0.89)
  the two profiles are of different devices: /device:TPU:13 before, /device:TPU:18 now
where the time goes in v2:
time: 53.9 us; the launch traced here: 53.8 us
  Pallas kernels  53.1 us (99%)
  between operations  0.64 us (1%)
    pallas_call x1, Pallas kernels, on_device(): pl.pallas_call(functools.partial(whole, devs, tps, seqs, own, heads, hd,...  51.2 us
    pallas_call x1, Pallas kernels, on_device(): pl.pallas_call(functools.partial(leave, len(results)), in_specs=[hbm] * l...  1.92 us

profile of v2, /device:TPU:18, one launch (start us, length us, event | category | flops | bytes accessed | tf_op | source)
XLA Modules:
  0.0 53.8 jit_solution(6747194746159511778)
XLA Ops:
  0.6 51.2 %shard_map.102 = (bf16[2,384,256]{2,1,0:T(8,128)(2,1)}, bf16[2,64,384]{2,1,0:T(8,128)(2,1)}, bf16[2,64,384]{2,1,0:T(8,128)(2,1)}, f32[128,256]{1,0:T(8,128)}) custom-call(s32[2,6,1,16]{3,2,1,0:T(1,128)} %chosen_ref.1, bf16[2,384,256]{2,1,0:T(8,128)(2,1)} %q_in.1, bf16[2,384,256]{2,1,0:T(8,128)(2,1)} %c_in.1, f32[2,4,384]{2,1,0:T(4,128)} %bitcast.7, ...), custom_call_target="tpu_custom_call" | custom-call | tf_op jit(solution)/shard_map/pallas_call | solution.py:453
  51.8 1.9 %shard_map.103 = (bf16[2,384,256]{2,1,0:T(8,128)(2,1)}, bf16[2,64,384]{2,1,0:T(8,128)(2,1)}, bf16[2,64,384]{2,1,0:T(8,128)(2,1)}, f32[128,256]{1,0:T(8,128)}) custom-call(bf16[2,384,256]{2,1,0:T(8,128)(2,1)} %get-tuple-element.12.refs_0_, bf16[2,64,384]{2,1,0:T(8,128)(2,1)} %get-tuple-element.13.refs_1_, bf16[2,64,384]{2,1,0:T(8,128)(2,1)} %get-tuple-element.14.refs_2_, ...), custom_call_target="tpu_custom_call" | custom-call | tf_op jit(solution)/shard_map/pallas_call | solution.py:511

commit v3 on v2

--- a/solution.py
+++ b/solution.py
@@ -11,8 +11,10 @@
 BLK = 64
 MOST = 2
 PAIR = 2
+DUO = 2
 SUB = 8
 LANES = 128
+SPAN = 2
 NEG = -1e30
 MESH = pl.DeviceIdType.MESH
 BF = jnp.bfloat16
@@ -37,10 +39,10 @@
     dq_out, kg_out, vo_out, wg_out,
     q_ref, c_ref, g_ref, k_ref, v_ref, dq_ref, kg_ref, vo_ref, wg_ref,
     near_ref, gate_ref, named_ref, hot_ref, asked_ref, farb_ref, nearb_ref,
-    reply_ref, far_ref, rows_ref, qs_ref, bg_ref, s_ref, w_ref, top_ref, dqt_ref,
-    out_ref, total_ref, back_ref, vg_ref, acc_ref, part_ref, piece_ref,
+    reply_ref, far_ref, rows_ref, qs_ref, bg_ref, s_ref, w_ref, top_ref, run_ref, dqt_ref,
+    out_ref, total_ref, back_ref, vg_ref, acc_ref, part_ref, mate_ref, both_ref, piece_ref,
     hot_send, hot_recv, far_send, far_recv, li_send, li_recv, li_sem,
-    back_send, back_recv, vg_send, vg_recv, piece_send, piece_recv, in_sem, out_sem,
+    back_send, back_recv, vg_send, vg_recv, toss_send, toss_recv, piece_send, piece_recv, in_sem, out_sem,
 ):
     me = lax.axis_index("kv")
     my_tp = lax.axis_index("tp")
@@ -105,11 +107,20 @@
             device_id={"tp": t}, device_id_type=MESH,
         )
 
-    def piece(kv, src):
-        return pltpu.make_async_remote_copy(
-            src_ref=part_ref.at[kv], dst_ref=piece_ref.at[src],
-            send_sem=piece_send.at[kv], recv_sem=piece_recv.at[src],
-            device_id={"kv": kv}, device_id_type=MESH,
+    halves, mine, my_u = devs // DUO, me // DUO, me % DUO
+
+    def toss(g):
+        return pltpu.make_async_remote_copy(
+            src_ref=part_ref.at[g * DUO + 1 - my_u], dst_ref=mate_ref.at[g],
+            send_sem=toss_send.at[g], recv_sem=toss_recv.at[g],
+            device_id={"kv": me + 1 - 2 * my_u}, device_id_type=MESH,
+        )
+
+    def piece(g, src):
+        return pltpu.make_async_remote_copy(
+            src_ref=both_ref.at[g], dst_ref=piece_ref.at[src],
+            send_sem=piece_send.at[g], recv_sem=piece_recv.at[src],
+            device_id={"kv": g * DUO + my_u}, device_id_type=MESH,
         )
 
     ins = [
@@ -164,7 +175,7 @@
     pl.semaphore_wait(barrier, devs - 1 + tps - 1)
     loop(0, me, lambda m: ask(m, me).start())
 
-    for copy in ins:
+    for copy in ins[:3]:
         copy.wait()
     for s in range(seqs):
         near_ref[s] = jnp.concatenate([k_ref[s], v_ref[s]], axis=0).T
@@ -193,11 +204,14 @@
         loop(0, groups, lambda g: shuffle(g, t, my_tp).start())
     loop(0, groups, lambda g: keep(g).start())
 
+    for copy in ins[3:]:
+        copy.wait()
     chunks = devs - 1
-    rows = heads * wide
+    span = SPAN * wide
+    blocks = [(t, h) for t in range(pairs) for h in range(heads // SPAN)]
     dims = (((1,), (1,)), ((), ()))
-    ahead = lax.broadcasted_iota(jnp.int32, (wide, rows), 0) <= lax.rem(
-        lax.broadcasted_iota(jnp.int32, (wide, rows), 1), wide
+    ahead = lax.broadcasted_iota(jnp.int32, (wide, span), 0) <= lax.rem(
+        lax.broadcasted_iota(jnp.int32, (wide, span), 1), wide
     )
 
     def settle(s):
@@ -219,57 +233,62 @@
         for t in peers:
             spread(s, t, my_tp).start()
 
-    def attention(s):
+    def score(s, kv, i, chunk, bias, diagonal, carry):
+        top, norm, dot = carry
+        cols = slice(i * span, (i + 1) * span)
+        raw = lax.dot_general(kv, qs_ref[s, i], dims, preferred_element_type=F32) * log2e
+        wg = lax.dot_general(kv, bg_ref[s, i], dims, preferred_element_type=F32)
+        sc = jnp.concatenate(
+            [
+                raw[j * BLK : (j + 1) * BLK] + jnp.concatenate([b] * SPAN, axis=1)
+                for j, b in enumerate(bias)
+            ],
+            axis=0,
+        )
+        if diagonal:
+            sc = jnp.where(ahead, sc, NEG)
+        peak = jnp.maximum(top, jnp.max(sc, axis=0, keepdims=True))
+        p = jnp.exp2(sc - peak)
+        less = jnp.exp2(top - peak)
+        s_ref[chunk, :, cols] = p.astype(s_ref.dtype)
+        w_ref[chunk, :, cols] = wg.astype(w_ref.dtype)
+        top_ref[chunk, :, cols] = peak
+        norm = norm * less + jnp.sum(p, axis=0, keepdims=True)
+        dot = dot * less + jnp.sum(p * wg, axis=0, keepdims=True)
+        return peak, norm, dot
+
+    def setup(s):
         for t in range(pairs):
             tok = slice(t * wide, (t + 1) * wide)
             q = (q_ref[s, tok, :].astype(F32) * scale).astype(BF)
             cot = c_ref[s, tok, :].astype(F32)
             gate = gate_ref[s, tok, :]
-            zero = jnp.zeros((rows, hd), BF)
-            qs = jnp.concatenate([q[:, h * hd : (h + 1) * hd] for h in range(heads)], axis=0)
-            bg = jnp.concatenate(
-                [gate[:, h : h + 1] * cot[:, h * hd : (h + 1) * hd] for h in range(heads)], axis=0
-            ).astype(BF)
-            qs_ref[t] = jnp.concatenate([qs, zero], axis=1)
-            bg_ref[t] = jnp.concatenate([zero, bg], axis=1)
-
-        def score(kv, t, chunk, bias, diagonal, carry):
-            top, norm, dot = carry
-            raw = lax.dot_general(kv, qs_ref[t], dims, preferred_element_type=F32) * log2e
-            wg = lax.dot_general(kv, bg_ref[t], dims, preferred_element_type=F32)
-            sc = jnp.concatenate(
-                [
-                    raw[j * BLK : (j + 1) * BLK] + jnp.concatenate([b] * heads, axis=1)
-                    for j, b in enumerate(bias)
-                ],
-                axis=0,
-            )
-            if diagonal:
-                sc = jnp.where(ahead, sc, NEG)
-            peak = jnp.maximum(top, jnp.max(sc, axis=0, keepdims=True))
-            p = jnp.exp2(sc - peak)
-            less = jnp.exp2(top - peak)
-            s_ref[chunk, :, t * rows : (t + 1) * rows] = p.astype(s_ref.dtype)
-            w_ref[chunk, :, t * rows : (t + 1) * rows] = wg
-            top_ref[chunk, :, t * rows : (t + 1) * rows] = peak
-            norm = norm * less + jnp.sum(p, axis=0, keepdims=True)
-            dot = dot * less + jnp.sum(p * wg, axis=0, keepdims=True)
-            return peak, norm, dot
-
-        carries = []
-        for t in range(pairs):
-            carry = (jnp.full((1, rows), NEG, F32), jnp.zeros((1, rows), F32), jnp.zeros((1, rows), F32))
+            zero = jnp.zeros((span, hd), BF)
+            for h in range(heads // SPAN):
+                hs = range(h * SPAN, (h + 1) * SPAN)
+                qs = jnp.concatenate([q[:, k * hd : (k + 1) * hd] for k in hs], axis=0)
+                bg = jnp.concatenate(
+                    [gate[:, k : k + 1] * cot[:, k * hd : (k + 1) * hd] for k in hs], axis=0
+                ).astype(BF)
+                i = t * (heads // SPAN) + h
+                qs_ref[s, i] = jnp.concatenate([qs, zero], axis=1)
+                bg_ref[s, i] = jnp.concatenate([zero, bg], axis=1)
+        for i, (t, h) in enumerate(blocks):
+            carry = (jnp.full((1, span), NEG, F32), jnp.zeros((1, span), F32), jnp.zeros((1, span), F32))
             for c in range(t, -1, -1):
                 kv = near_ref[s, c * wide : (c + 1) * wide, :]
                 bias = [
                     nearb_ref[s * pairs + t, c * PAIR + j : c * PAIR + j + 1, :] for j in range(PAIR)
                 ]
-                carry = score(kv, t, chunks + c, bias, c == t, carry)
-            carries.append(carry)
-
-        @pl.when(s == 0)
-        def _():
-            loop(nearest, later, first)
+                carry = score(s, kv, i, chunks + s * pairs + c, bias, c == t, carry)
+            for k in range(3):
+                run_ref[s, k, :, i * span : (i + 1) * span] = carry[k]
+
+    def attention(s):
+        carries = tuple(
+            tuple(run_ref[s, k, :, i * span : (i + 1) * span] for k in range(3))
+            for i in range(len(blocks))
+        )
 
         def forth(i, carries):
             m = me - 1 - i
@@ -277,18 +296,14 @@
             kv = far_ref[s, m]
             return tuple(
                 score(
-                    kv, t, m,
+                    s, kv, i, m,
                     [farb_ref[s * pairs + t, j, pl.ds(m, 1), :] for j in range(MOST)],
-                    False, carries[t],
+                    False, carries[i],
                 )
-                for t in range(pairs)
+                for i, (t, h) in enumerate(blocks)
             )
 
-        carries = lax.fori_loop(0, me, forth, tuple(carries))
-
-        @pl.when((s < seqs - 1) & (me * 2 >= devs))
-        def _():
-            loop(0, later, functools.partial(reply, s + 1))
+        carries = lax.fori_loop(0, me, forth, carries)
 
         @pl.when(s > 0)
         def _():
@@ -299,37 +314,42 @@
         dots = [carry[2] * inv for carry, inv in zip(carries, invs)]
         dqt_ref[...] = jnp.zeros_like(dqt_ref)
 
-        def grad(kv, chunk, ts):
+        def grad(kv, chunk, first_t):
             kt = (kv[:, :hd] * scale).astype(BF).T
             total = None
-            for t in ts:
-                cols = slice(t * rows, (t + 1) * rows)
-                part = jnp.exp2(top_ref[chunk, :, cols] - tops[t]) * invs[t]
+            for i, (t, h) in enumerate(blocks):
+                if t < first_t:
+                    continue
+                cols = slice(i * span, (i + 1) * span)
+                part = jnp.exp2(top_ref[chunk, :, cols] - tops[i]) * invs[i]
                 w = s_ref[chunk, :, cols].astype(F32) * part
-                ds = (w * (w_ref[chunk, :, cols] - dots[t])).astype(BF)
-                more = jnp.dot(ds, qs_ref[t], preferred_element_type=F32)
-                more += jnp.dot(w.astype(BF), bg_ref[t], preferred_element_type=F32)
+                ds = (w * (w_ref[chunk, :, cols].astype(F32) - dots[i])).astype(BF)
+                more = jnp.dot(ds, qs_ref[s, i], preferred_element_type=F32)
+                more += jnp.dot(w.astype(BF), bg_ref[s, i], preferred_element_type=F32)
                 total = more if total is None else total + more
                 dqt_ref[:, cols] += jnp.dot(kt, ds, preferred_element_type=F32)
             return total
 
         def give(m):
-            out_ref[s, m] = grad(far_ref[s, m], m, range(pairs)).astype(BF)
+            out_ref[s, m] = grad(far_ref[s, m], m, 0).astype(BF)
             back(s, m, me).start()
 
         loop(0, me, give)
         for c in range(pairs):
             kv = near_ref[s, c * wide : (c + 1) * wide, :]
-            total_ref[s, c * wide : (c + 1) * wide, :] = grad(kv, chunks + c, range(c, pairs))
+            total_ref[s, c * wide : (c + 1) * wide, :] = grad(kv, chunks + s * pairs + c, c)
         for t in range(pairs):
-            dqt = dqt_ref[:, t * rows : (t + 1) * rows]
-            dqt = jnp.concatenate([dqt[:, h * wide : (h + 1) * wide] for h in range(heads)], axis=0)
+            dqt = jnp.concatenate(
+                [dqt_ref[:, (t * heads + h) * wide : (t * heads + h + 1) * wide] for h in range(heads)],
+                axis=0,
+            )
             dq_ref[s, t * wide : (t + 1) * wide, :] = dqt.T.astype(BF)
 
-        @pl.when((s < seqs - 1) & (me * 2 < devs))
-        def _():
-            loop(0, later, functools.partial(reply, s + 1))
-
+    setup(0)
+    loop(nearest, later, first)
+    for s in range(1, seqs):
+        setup(s)
+        loop(0, later, functools.partial(reply, s))
     loop(0, seqs, attention)
     puts = [put(0, dq_ref, dq_out)]
     puts[0].start()
@@ -337,21 +357,24 @@
     def product(s, g):
         return jnp.dot(vg_ref[s], rows_ref[g, s], preferred_element_type=F32)
 
+    def begin():
+        for t in peers:
+            loop(0, groups, lambda g: shuffle(g, t, t).wait_recv())
+        loop(0, groups, lambda g: keep(g).wait())
+        for s in range(seqs - 1):
+            for t in peers:
+                spread(s, t, t).wait_recv()
+
+            def early(g):
+                if s == 0:
+                    acc_ref[g] = product(s, g)
+                else:
+                    acc_ref[g] += product(s, g)
+
+            loop(0, groups, early)
+
     settle(seqs - 1)
-    for t in peers:
-        loop(0, groups, lambda g: shuffle(g, t, t).wait_recv())
-    loop(0, groups, lambda g: keep(g).wait())
-    for s in range(seqs - 1):
-        for t in peers:
-            spread(s, t, t).wait_recv()
-
-        def early(g):
-            if s == 0:
-                acc_ref[g] = product(s, g)
-            else:
-                acc_ref[g] += product(s, g)
-
-        loop(0, groups, early)
+    begin()
 
     for out in [put(1, kg_ref, kg_out), put(2, vo_ref, vo_out)]:
         out.start()
@@ -360,10 +383,10 @@
         spread(seqs - 1, t, t).wait_recv()
 
     def other(i):
-        low = devs - 1 - i
-        low = jnp.where(low > me, low, low - 1)
-        high = jnp.where(i < me, i, i + 1)
-        return jnp.where(me * 2 < devs, low, high)
+        low = halves - 1 - i
+        low = jnp.where(low > mine, low, low - 1)
+        high = jnp.where(i < mine, i, i + 1)
+        return jnp.where(i == halves - 1, mine, jnp.where(mine * 2 < halves, low, high))
 
     def final(g):
         last = product(seqs - 1, g)
@@ -372,12 +395,11 @@
     if groups == devs:
 
         def stage(i):
-            kv = other(i)
-            part_ref[kv] = final(kv).astype(BF)
-            piece(kv, me).start()
-
-        loop(0, devs - 1, stage)
-        part_ref[me] = final(me).astype(BF)
+            g = other(i)
+            part_ref[g * DUO + 1 - my_u] = final(g * DUO + 1 - my_u).astype(BF)
+            toss(g).start()
+
+        loop(0, halves, stage)
     else:
         each = devs // groups
 
@@ -385,15 +407,26 @@
             part_ref[pl.ds(g * each, each)] = final(g).T.astype(BF).reshape((each,) + part_ref.shape[1:])
 
         loop(0, groups, stage)
-        loop(0, devs - 1, lambda i: piece(other(i), me).start())
-    piece_ref[me] = part_ref[me]
-
-    def arrive(i):
-        piece(0, other(i)).wait_recv()
-
-    loop(0, devs - 1, arrive)
+        loop(0, halves, lambda i: toss(other(i)).start())
+
+    def merge(i):
+        g = other(i)
+        if groups == devs:
+            here = final(g * DUO + my_u)
+        else:
+            here = part_ref[g * DUO + my_u].astype(F32)
+        toss(g).wait_recv()
+        both_ref[g] = (here + mate_ref[g].astype(F32)).astype(BF)
+
+        @pl.when(i < halves - 1)
+        def _():
+            piece(g, mine).start()
+
+    loop(0, halves, merge)
+    piece_ref[mine] = both_ref[mine]
+    loop(0, halves - 1, lambda i: piece(other(i), other(i)).wait_recv())
     result = piece_ref[0].astype(F32)
-    for n in range(1, devs):
+    for n in range(1, halves):
         result += piece_ref[n].astype(F32)
     wg_ref[...] = result.T if groups == devs else result
     puts.append(put(3, wg_ref, wg_out))
@@ -407,7 +440,8 @@
         loop(0, me, lambda m: back(s, m, me).wait_send())
         for t in peers:
             spread(s, t, my_tp).wait_send()
-    loop(0, devs - 1, lambda i: piece(other(i), me).wait_send())
+    loop(0, halves, lambda i: toss(i).wait_send())
+    loop(0, halves - 1, lambda i: piece(other(i), mine).wait_send())
     for out in puts:
         out.wait()
 
@@ -436,13 +470,14 @@
     tps = lax.axis_size("tp")
     pos = layer_input.shape[1]
     share = layer_input.shape[2] // (devs * tps)
+    halves = devs // DUO
     groups, cut = devs, share
     if share % LANES:
         groups, cut = devs * share // LANES, LANES
         layer_input = layer_input.reshape(seqs, pos, devs, tps, share)
         layer_input = jnp.swapaxes(layer_input, 2, 3).reshape(seqs, pos, devs * tps * share)
     part = (tps * hd, share) if groups == devs else (share, tps * hd)
-    chunks = devs - 1 + pairs
+    chunks = devs - 1 + seqs * pairs
     rows = heads * PAIR * BLK
     scores = (chunks, PAIR * BLK, pairs * rows)
     sent = (MOST * BLK, 2 * hd)
@@ -480,11 +515,12 @@
             pltpu.VMEM((seqs, devs) + sent, BF),
             pltpu.VMEM((seqs, devs - 1) + sent, BF),
             pltpu.VMEM((groups, seqs, toks, cut), BF),
-            pltpu.VMEM((pairs, rows, 2 * hd), BF),
-            pltpu.VMEM((pairs, rows, 2 * hd), BF),
+            pltpu.VMEM((seqs, pairs * heads // SPAN, SPAN * PAIR * BLK, 2 * hd), BF),
+            pltpu.VMEM((seqs, pairs * heads // SPAN, SPAN * PAIR * BLK, 2 * hd), BF),
             pltpu.VMEM(scores, F32 if math.prod(scores) <= 5 * 2**20 else BF),
-            pltpu.VMEM(scores, F32),
+            pltpu.VMEM(scores, F32 if math.prod(scores) <= 5 * 2**20 else BF),
             pltpu.VMEM((chunks, 1, pairs * rows), F32),
+            pltpu.VMEM((seqs, 3, 1, pairs * rows), F32),
             pltpu.VMEM((hd, pairs * rows), F32),
             pltpu.VMEM((seqs, devs - 1) + sent, BF),
             pltpu.VMEM((seqs, toks, 2 * hd), F32),
@@ -492,13 +528,16 @@
             pltpu.VMEM((seqs, tps * hd, toks), BF),
             pltpu.VMEM((groups, tps * hd, cut), F32),
             pltpu.VMEM((devs,) + part, BF),
-            pltpu.VMEM((devs,) + part, BF),
+            pltpu.VMEM((halves,) + part, BF),
+            pltpu.VMEM((halves,) + part, BF),
+            pltpu.VMEM((halves,) + part, BF),
             dma((devs,)), dma((devs,)),
             dma((seqs, devs)), dma((seqs, devs)),
             dma((tps, groups)), dma((tps, groups)), dma((groups,)),
             dma((seqs, devs)), dma((seqs, devs)),
             dma((seqs, tps)), dma((seqs, tps)),
-            dma((devs,)), dma((devs,)),
+            dma((halves,)), dma((halves,)),
+            dma((halves,)), dma((halves,)),
             dma((5,)), dma((4,)),
         ],
         compiler_params=pltpu.CompilerParams(

time: 53.9 us -> 51.5 us (0.955)
  the two profiles are of different devices: /device:TPU:18 before, /device:TPU:0 now
where the time goes in v3:
time: 51.5 us; the launch traced here: 51.3 us
  Pallas kernels  50.7 us (98%)
  between operations  0.64 us (1%)
    pallas_call x1, Pallas kernels, on_device(): pl.pallas_call(functools.partial(whole, devs, tps, seqs, own, heads, hd,...  48.7 us
    pallas_call x1, Pallas kernels, on_device(): pl.pallas_call(functools.partial(leave, len(results)), in_specs=[hbm] * l...  1.92 us

profile of v3, /device:TPU:0, one launch (start us, length us, event | category | flops | bytes accessed | tf_op | source)
XLA Modules:
  0.0 51.3 jit_solution(13857630904537129258)
XLA Ops:
  0.6 48.7 %shard_map.102 = (bf16[2,384,256]{2,1,0:T(8,128)(2,1)}, bf16[2,64,384]{2,1,0:T(8,128)(2,1)}, bf16[2,64,384]{2,1,0:T(8,128)(2,1)}, f32[128,256]{1,0:T(8,128)}) custom-call(s32[2,6,1,16]{3,2,1,0:T(1,128)} %chosen_ref.1, bf16[2,384,256]{2,1,0:T(8,128)(2,1)} %q_in.1, bf16[2,384,256]{2,1,0:T(8,128)(2,1)} %c_in.1, f32[2,4,384]{2,1,0:T(4,128)} %bitcast.7, ...), custom_call_target="tpu_custom_call" | custom-call | tf_op jit(solution)/shard_map/pallas_call | solution.py:488
  49.4 1.9 %shard_map.103 = (bf16[2,384,256]{2,1,0:T(8,128)(2,1)}, bf16[2,64,384]{2,1,0:T(8,128)(2,1)}, bf16[2,64,384]{2,1,0:T(8,128)(2,1)}, f32[128,256]{1,0:T(8,128)}) custom-call(bf16[2,384,256]{2,1,0:T(8,128)(2,1)} %get-tuple-element.12.refs_0_, bf16[2,64,384]{2,1,0:T(8,128)(2,1)} %get-tuple-element.13.refs_1_, bf16[2,64,384]{2,1,0:T(8,128)(2,1)} %get-tuple-element.14.refs_2_, ...), custom_call_target="tpu_custom_call" | custom-call | tf_op jit(solution)/shard_map/pallas_call | solution.py:550

commit v4 on v3

--- a/solution.py
+++ b/solution.py
@@ -34,12 +34,12 @@
 
 
 def whole(
-    devs, tps, seqs, own, heads, hd, share, groups,
+    devs, tps, seqs, own, heads, hd, share, groups, defer,
     chosen_ref, q_in, c_in, g_in, k_in, v_in, li_ref,
     dq_out, kg_out, vo_out, wg_out,
     q_ref, c_ref, g_ref, k_ref, v_ref, dq_ref, kg_ref, vo_ref, wg_ref,
     near_ref, gate_ref, named_ref, hot_ref, asked_ref, farb_ref, nearb_ref,
-    reply_ref, far_ref, rows_ref, qs_ref, bg_ref, s_ref, w_ref, top_ref, run_ref, dqt_ref,
+    reply_ref, far_ref, rows_ref, qs_ref, bg_ref, s_ref, w_ref, ds_ref, top_ref, run_ref, dqt_ref,
     out_ref, total_ref, back_ref, vg_ref, acc_ref, part_ref, mate_ref, both_ref, piece_ref,
     hot_send, hot_recv, far_send, far_recv, li_send, li_recv, li_sem,
     back_send, back_recv, vg_send, vg_recv, toss_send, toss_recv, piece_send, piece_recv, in_sem, out_sem,
@@ -312,10 +312,11 @@
         tops = [carry[0] for carry in carries]
         invs = [1.0 / carry[1] for carry in carries]
         dots = [carry[2] * inv for carry, inv in zip(carries, invs)]
-        dqt_ref[...] = jnp.zeros_like(dqt_ref)
-
-        def grad(kv, chunk, first_t):
-            kt = (kv[:, :hd] * scale).astype(BF).T
+        if not defer:
+            dqt_ref[...] = jnp.zeros_like(dqt_ref)
+
+        def grad(kv, chunk, slot, first_t):
+            kt = None if defer else (kv[:, :hd] * scale).astype(BF).T
             total = None
             for i, (t, h) in enumerate(blocks):
                 if t < first_t:
@@ -327,17 +328,32 @@
                 more = jnp.dot(ds, qs_ref[s, i], preferred_element_type=F32)
                 more += jnp.dot(w.astype(BF), bg_ref[s, i], preferred_element_type=F32)
                 total = more if total is None else total + more
-                dqt_ref[:, cols] += jnp.dot(kt, ds, preferred_element_type=F32)
+                if defer:
+                    ds_ref[slot, :, cols] = ds
+                else:
+                    dqt_ref[:, cols] += jnp.dot(kt, ds, preferred_element_type=F32)
             return total
 
-        def give(m):
-            out_ref[s, m] = grad(far_ref[s, m], m, 0).astype(BF)
+        def give(i):
+            m = jnp.where(me < 2 * quarter, i, order(i))
+            out_ref[s, m] = grad(far_ref[s, m], m, s * (chunks + pairs) + m, 0).astype(BF)
             back(s, m, me).start()
 
         loop(0, me, give)
         for c in range(pairs):
             kv = near_ref[s, c * wide : (c + 1) * wide, :]
-            total_ref[s, c * wide : (c + 1) * wide, :] = grad(kv, chunks + s * pairs + c, c)
+            total_ref[s, c * wide : (c + 1) * wide, :] = grad(
+                kv, chunks + s * pairs + c, s * (chunks + pairs) + chunks + c, c
+            )
+        if not defer:
+            turn(s)
+
+    quarter = devs // 4
+
+    def order(i):
+        return jnp.where(i < quarter, i + quarter, jnp.where(i < 2 * quarter, i - quarter, i))
+
+    def turn(s):
         for t in range(pairs):
             dqt = jnp.concatenate(
                 [dqt_ref[:, (t * heads + h) * wide : (t * heads + h + 1) * wide] for h in range(heads)],
@@ -345,14 +361,35 @@
             )
             dq_ref[s, t * wide : (t + 1) * wide, :] = dqt.T.astype(BF)
 
+    def query_side(s):
+        first = s * (chunks + pairs)
+        for c in range(pairs):
+            kt = (near_ref[s, c * wide : (c + 1) * wide, :hd] * scale).astype(BF).T
+            for i, (t, h) in enumerate(blocks):
+                if t >= c:
+                    cols = slice(i * span, (i + 1) * span)
+                    more = jnp.dot(kt, ds_ref[first + chunks + c, :, cols], preferred_element_type=F32)
+                    if c == 0:
+                        dqt_ref[:, cols] = more
+                    else:
+                        dqt_ref[:, cols] += more
+
+        def far_side(m):
+            kt = (far_ref[s, m][:, :hd] * scale).astype(BF).T
+            for i in range(len(blocks)):
+                cols = slice(i * span, (i + 1) * span)
+                dqt_ref[:, cols] += jnp.dot(kt, ds_ref[first + m, :, cols], preferred_element_type=F32)
+
+        loop(0, me, far_side)
+        turn(s)
+
     setup(0)
     loop(nearest, later, first)
     for s in range(1, seqs):
         setup(s)
         loop(0, later, functools.partial(reply, s))
     loop(0, seqs, attention)
-    puts = [put(0, dq_ref, dq_out)]
-    puts[0].start()
+    puts = []
 
     def product(s, g):
         return jnp.dot(vg_ref[s], rows_ref[g, s], preferred_element_type=F32)
@@ -422,6 +459,10 @@
         def _():
             piece(g, mine).start()
 
+    if defer:
+        loop(0, seqs, query_side)
+    puts.append(put(0, dq_ref, dq_out))
+    puts[-1].start()
     loop(0, halves, merge)
     piece_ref[mine] = both_ref[mine]
     loop(0, halves - 1, lambda i: piece(other(i), other(i)).wait_recv())
@@ -480,13 +521,15 @@
     chunks = devs - 1 + seqs * pairs
     rows = heads * PAIR * BLK
     scores = (chunks, PAIR * BLK, pairs * rows)
+    kept = (seqs * (devs - 1 + pairs),) + scores[1:]
+    defer = math.prod(kept) <= 5 * 2**20
     sent = (MOST * BLK, 2 * hd)
 
     vmem = pl.BlockSpec(memory_space=pltpu.VMEM)
     hbm = pl.BlockSpec(memory_space=pl.ANY)
     dma = pltpu.SemaphoreType.DMA
     results = pl.pallas_call(
-        functools.partial(whole, devs, tps, seqs, own, heads, hd, cut, groups),
+        functools.partial(whole, devs, tps, seqs, own, heads, hd, cut, groups, defer),
         in_specs=[vmem] + [hbm] * 6,
         out_specs=[hbm] * 4,
         out_shape=[
@@ -519,6 +562,7 @@
             pltpu.VMEM((seqs, pairs * heads // SPAN, SPAN * PAIR * BLK, 2 * hd), BF),
             pltpu.VMEM(scores, F32 if math.prod(scores) <= 5 * 2**20 else BF),
             pltpu.VMEM(scores, F32 if math.prod(scores) <= 5 * 2**20 else BF),
+            pltpu.VMEM(kept if defer else (1, SUB, LANES), BF),
             pltpu.VMEM((chunks, 1, pairs * rows), F32),
             pltpu.VMEM((seqs, 3, 1, pairs * rows), F32),
             pltpu.VMEM((hd, pairs * rows), F32),

time: 51.5 us -> 50.7 us (0.984)
  Pallas kernels: 50.7 us -> 49.8 us
    pallas_call x1, Pallas kernels: 48.7 us -> 47.9 us  [on_device(): pl.pallas_call(functools.partial(whole, devs, tps, seqs, own, heads, hd,...]
where the time goes in v4:
time: 50.7 us; the launch traced here: 50.5 us
  Pallas kernels  49.8 us (98%)
  between operations  0.64 us (1%)
    pallas_call x1, Pallas kernels, on_device(): pl.pallas_call(functools.partial(whole, devs, tps, seqs, own, heads, hd,...  47.9 us
    pallas_call x1, Pallas kernels, on_device(): pl.pallas_call(functools.partial(leave, len(results)), in_specs=[hbm] * l...  1.92 us

profile of v4, /device:TPU:0, one launch (start us, length us, event | category | flops | bytes accessed | tf_op | source)
XLA Modules:
  0.0 50.5 jit_solution(8548758979444021125)
XLA Ops:
  0.6 47.9 %shard_map.102 = (bf16[2,384,256]{2,1,0:T(8,128)(2,1)}, bf16[2,64,384]{2,1,0:T(8,128)(2,1)}, bf16[2,64,384]{2,1,0:T(8,128)(2,1)}, f32[128,256]{1,0:T(8,128)}) custom-call(s32[2,6,1,16]{3,2,1,0:T(1,128)} %chosen_ref.1, bf16[2,384,256]{2,1,0:T(8,128)(2,1)} %q_in.1, bf16[2,384,256]{2,1,0:T(8,128)(2,1)} %c_in.1, f32[2,4,384]{2,1,0:T(4,128)} %bitcast.7, ...), custom_call_target="tpu_custom_call" | custom-call | tf_op jit(solution)/shard_map/pallas_call | solution.py:531
  48.6 1.9 %shard_map.103 = (bf16[2,384,256]{2,1,0:T(8,128)(2,1)}, bf16[2,64,384]{2,1,0:T(8,128)(2,1)}, bf16[2,64,384]{2,1,0:T(8,128)(2,1)}, f32[128,256]{1,0:T(8,128)}) custom-call(bf16[2,384,256]{2,1,0:T(8,128)(2,1)} %get-tuple-element.12.refs_0_, bf16[2,64,384]{2,1,0:T(8,128)(2,1)} %get-tuple-element.13.refs_1_, bf16[2,64,384]{2,1,0:T(8,128)(2,1)} %get-tuple-element.14.refs_2_, ...), custom_call_target="tpu_custom_call" | custom-call | tf_op jit(solution)/shard_map/pallas_call | solution.py:594
